TPU v7x, 128 devices: a whole 4x4x4 slice. The times are simulated.
128 devices in a mesh: sp: 32 (over z, y, core), tp: 4 (over x).
Axes of the slice: x: 4, y: 4, z: 4, core: 2. Of those that a mesh axis runs over, the one named last changes fastest.
Arguments:
- query_nope: bfloat16 [6144, 4096], P('sp', 'tp'), may hold values from -6 to 6
- query_rope: bfloat16 [6144, 2048], P('sp', 'tp'), may hold values from -24 to 24
- latent: bfloat16 [6144, 512], P('sp'), may hold values from -6 to 6
- key_rope: bfloat16 [6144, 32], P('sp'), may hold values from -24 to 24
- latent_gain: float32 [512], replicated, may hold values from 0.1 to 1.9
- key_up: bfloat16 [512, 4096], P(None, 'tp'), may hold values from -0.25 to 0.25
- value_up: bfloat16 [512, 4096], P(None, 'tp'), may hold values from -0.25 to 0.25
- out_proj: bfloat16 [4096, 4096], P('tp'), may hold values from -0.09375 to 0.09375
- resid: bfloat16 [6144, 4096], P(('sp', 'tp')), may hold values from -6 to 6
- attn_gain: float32 [4096], replicated, may hold values from 0.1 to 1.9
- pre_gain: float32 [4096], replicated, may hold values from 0.1 to 1.9
- routes: int32 [6144, 2], P(('sp', 'tp')), may hold values from 0 to 31, all different within a row; in each aligned block of 48 rows (0 to 47, 48 to 95, ...) at most 6 rows name the same one
- route_weights: float32 [6144, 2], P(('sp', 'tp')), may hold values from 0.2 to 2
- expert_gate: bfloat16 [32, 4096, 1024], P('sp', None, 'tp'), may hold values from -0.09375 to 0.09375
- expert_up: bfloat16 [32, 4096, 1024], P('sp', None, 'tp'), may hold values from -0.09375 to 0.09375
- expert_down: bfloat16 [32, 1024, 4096], P('sp', 'tp'), may hold values from -0.1875 to 0.1875
- shared_gate: bfloat16 [4096, 1024], P(None, 'tp'), may hold values from -0.09375 to 0.09375
- shared_up: bfloat16 [4096, 1024], P(None, 'tp'), may hold values from -0.09375 to 0.09375
- shared_down: bfloat16 [1024, 4096], P('tp'), may hold values from -0.1875 to 0.1875
- moe_gain: float32 [4096], replicated, may hold values from 0.1 to 1.9
Outputs:
- output: bfloat16 [6144, 4096], P(('sp', 'tp'))
Inputs may be any that keep to these rules, and one draw needn't show every extreme that they name: `routes`: A row names 2 different experts. In each aligned block of 48 rows no expert is named by more than 6 rows, and in some block an expert is named by exactly 6 rows.
All inputs are finite; a program needn't handle non-finite values.
Results may differ from a plain program's by a relative error of at most 0.018.
Values may be sent and summed in bfloat16 or wider, within the bound.
No kernel may reach another device: no remote copies, remote signals or barrier semaphores. Data moves between devices by JAX's collectives and lax.ppermute only.
A program may use at most 128 MiB of HBM per device.

v0:
```python
import math
import jax
import jax.numpy as jnp
from jax import lax
from jax.sharding import PartitionSpec as P

MODEL_DIM = 4096
NOPE_DIM = 64
ROPE_DIM = 32
VALUE_DIM = 64
TOP_K = 2
epsilon = 1e-06
theta_base = 10000.0


def cut_along(array, dim, count):
    before, after = (array.shape[:dim], array.shape[dim + 1 :])
    return jnp.moveaxis(array.reshape(*before, count, -1, *after), dim, 0)


def sum_at_owner(array, axis, dim):
    count = lax.axis_size(axis)
    blocks = lax.all_to_all(cut_along(array, dim, count), axis, 0, 0, tiled=True)
    return jnp.sum(blocks.astype(jnp.float32), axis=0)


def rms_scale(values, gain_vector):
    return (
        values
        * lax.rsqrt(jnp.mean(values * values, axis=-1, keepdims=True) + epsilon)
        * gain_vector
    )


def rotate(values, positions):
    half_dim = values.shape[-1] // 2
    inverse = theta_base ** (-jnp.arange(half_dim, dtype=jnp.float32) / half_dim)
    angles = positions.astype(jnp.float32)[..., None] * inverse
    cosine = jnp.cos(angles)
    sine_part = jnp.sin(angles)
    first_half = values[..., :half_dim]
    second_half = values[..., half_dim:]
    return jnp.concatenate(
        [
            first_half * cosine - second_half * sine_part,
            second_half * cosine + first_half * sine_part,
        ],
        axis=-1,
    )


def expert_block(expert_in, gate_part, up_part, down_part):
    hidden = (
        jax.nn.silu(jnp.dot(expert_in, gate_part, preferred_element_type=jnp.float32))
        * jnp.dot(expert_in, up_part, preferred_element_type=jnp.float32)
    ).astype(jnp.bfloat16)
    return jnp.dot(hidden, down_part, preferred_element_type=jnp.float32).astype(jnp.bfloat16)


def dispatch_table(normed_rows, route_rows, experts, capacity):
    row_count = normed_rows.shape[0]
    flat_routes = route_rows.reshape(-1)
    onehot = (flat_routes[:, None] == jnp.arange(experts, dtype=jnp.int32)[None, :]).astype(
        jnp.int32
    )
    earlier = jnp.cumsum(onehot, axis=0) - onehot
    target = flat_routes * capacity + jnp.sum(earlier * onehot, axis=1)
    matches = (
        target.reshape(row_count, -1)[None, :, :]
        == jnp.arange(experts * capacity, dtype=jnp.int32)[:, None, None]
    )
    spread = jnp.any(matches, axis=2).astype(jnp.bfloat16)
    slot_table = jnp.dot(spread, normed_rows, preferred_element_type=jnp.float32).astype(
        jnp.bfloat16
    )
    return (slot_table.reshape(experts, capacity, normed_rows.shape[1]), target)


def on_device(
    query_nope,
    query_rope,
    latent,
    key_rope,
    latent_gain,
    key_up,
    value_up,
    out_proj,
    resid,
    attn_gain,
    pre_gain,
    routes,
    route_weights,
    expert_gate,
    expert_up,
    expert_down,
    shared_gate,
    shared_up,
    shared_down,
    moe_gain,
):
    local_rows = query_nope.shape[0]
    heads_here = query_nope.shape[1] // NOPE_DIM
    query_pos = lax.axis_index("sp") * local_rows + jnp.arange(local_rows, dtype=jnp.int32)
    last_query = lax.axis_index("sp") * local_rows + local_rows - 1
    query_rot = rotate(
        query_rope.astype(jnp.float32).reshape(local_rows, heads_here, ROPE_DIM), query_pos[:, None]
    ).astype(jnp.bfloat16)
    key_rot = rotate(key_rope.astype(jnp.float32), query_pos).astype(jnp.bfloat16)
    latent_normed = rms_scale(latent.astype(jnp.float32), latent_gain).astype(jnp.bfloat16)
    query_heads = query_nope.reshape(local_rows, heads_here, NOPE_DIM)
    score_scale = (NOPE_DIM + ROPE_DIM) ** (-0.5)

    def attend(state_now, latent_rows, rotary_rows, key_start):
        piece_rows = latent_rows.shape[0]
        keys_here = jnp.dot(latent_rows, key_up, preferred_element_type=jnp.float32).astype(
            jnp.bfloat16
        )
        keys_here = keys_here.reshape(piece_rows, heads_here, NOPE_DIM)
        values_here = jnp.dot(latent_rows, value_up, preferred_element_type=jnp.float32).astype(
            jnp.bfloat16
        )
        values_here = values_here.reshape(piece_rows, heads_here, VALUE_DIM)
        scores = (
            jnp.einsum("qhd,khd->hqk", query_heads, keys_here, preferred_element_type=jnp.float32)
            + jnp.einsum("qhr,kr->hqk", query_rot, rotary_rows, preferred_element_type=jnp.float32)
        ) * score_scale
        allowed = (key_start + jnp.arange(piece_rows, dtype=jnp.int32))[None, :] <= query_pos[
            :, None
        ]
        scores = jnp.where(allowed[None], scores, -1e30)
        running, total_sum, summed = state_now
        newest = jnp.maximum(running, jnp.max(scores, axis=-1))
        factor = jnp.exp(running - newest)
        exponent = jnp.exp(scores - newest[..., None])
        total_sum = total_sum * factor + jnp.sum(exponent, axis=-1)
        summed = summed * factor[..., None] + jnp.einsum(
            "hqk,khd->hqd",
            exponent.astype(jnp.bfloat16),
            values_here,
            preferred_element_type=jnp.float32,
        )
        return (newest, total_sum, summed)

    initial = (
        jnp.full((heads_here, local_rows), -1e30, jnp.float32),
        jnp.zeros((heads_here, local_rows), jnp.float32),
        jnp.zeros((heads_here, local_rows, VALUE_DIM), jnp.float32),
    )
    latent_piece = lax.all_gather(latent_normed, "sp", axis=0, tiled=True)
    rotary_piece = lax.all_gather(key_rot, "sp", axis=0, tiled=True)
    piece_rows = latent_piece.shape[0]
    step_rows = math.gcd(piece_rows, 512)

    def one_step(step_index, inner_state):
        offset = step_index * step_rows
        latent_rows = lax.dynamic_slice_in_dim(latent_piece, offset, step_rows, 0)
        rotary_rows = lax.dynamic_slice_in_dim(rotary_piece, offset, step_rows, 0)
        return lax.cond(
            offset <= last_query,
            lambda carried: attend(carried, latent_rows, rotary_rows, offset),
            lambda carried: carried,
            inner_state,
        )

    running, total_sum, summed = lax.fori_loop(0, piece_rows // step_rows, one_step, initial)
    attention = (
        (summed / total_sum[..., None])
        .transpose(1, 0, 2)
        .reshape(local_rows, heads_here * VALUE_DIM)
    )
    attention = attention.astype(jnp.bfloat16)
    projected = sum_at_owner(
        jnp.dot(attention, out_proj, preferred_element_type=jnp.float32).astype(jnp.bfloat16),
        "tp",
        0,
    )
    mixed = (resid.astype(jnp.float32) + rms_scale(projected, attn_gain)).astype(jnp.bfloat16)
    normed = rms_scale(mixed.astype(jnp.float32), pre_gain).astype(jnp.bfloat16)
    rows_here = resid.shape[0]
    tp_count = lax.axis_size("tp")
    experts = lax.axis_size("sp")
    capacity = max(2, 2 * rows_here * TOP_K // experts)
    own_table, target = dispatch_table(normed, routes, experts, capacity)
    arrived = lax.all_to_all(own_table, "sp", split_axis=0, concat_axis=0, tiled=True)
    column = lax.all_gather(arrived[None], "tp", axis=0, tiled=True)
    group_normed = lax.all_gather(normed, "tp", axis=0, tiled=True)
    expert_out = expert_block(
        column.reshape(-1, MODEL_DIM), expert_gate[0], expert_up[0], expert_down[0]
    )
    shared_part = expert_block(group_normed, shared_gate, shared_up, shared_down)
    routed_sum, shared_sum = (
        lax.psum_scatter(
            expert_out.reshape(column.shape).astype(jnp.float32).astype(jnp.bfloat16),
            "tp",
            scatter_dimension=0,
            tiled=True,
        ).astype(jnp.float32),
        lax.psum_scatter(
            shared_part.reshape(tp_count, rows_here, MODEL_DIM)
            .astype(jnp.float32)
            .astype(jnp.bfloat16),
            "tp",
            scatter_dimension=0,
            tiled=True,
        ).astype(jnp.float32),
    )
    expert_rows = lax.all_to_all(
        routed_sum.astype(jnp.bfloat16), "sp", split_axis=1, concat_axis=1, tiled=True
    ).reshape(-1, MODEL_DIM)
    shared_out = shared_sum.reshape(rows_here, MODEL_DIM)
    picked = expert_rows[target].astype(jnp.float32).reshape(rows_here, TOP_K, MODEL_DIM)
    routed = jnp.sum(picked * route_weights[..., None], axis=1)
    moe = shared_out + routed
    return (mixed.astype(jnp.float32) + rms_scale(moe, moe_gain)).astype(jnp.bfloat16)


def solution(mesh):
    in_specs = (
        P("sp", "tp"),
        P("sp", "tp"),
        P("sp", None),
        P("sp", None),
        P(),
        P(None, "tp"),
        P(None, "tp"),
        P("tp", None),
        P(("sp", "tp"), None),
        P(),
        P(),
        P(("sp", "tp"), None),
        P(("sp", "tp"), None),
        P("sp", None, "tp"),
        P("sp", None, "tp"),
        P("sp", "tp", None),
        P(None, "tp"),
        P(None, "tp"),
        P("tp", None),
        P(),
    )
    out_specs = P(("sp", "tp"), None)
    return jax.shard_map(
        on_device, mesh=mesh, in_specs=in_specs, out_specs=out_specs, check_vma=False
    )
```

profile of v0, /device:TPU:0, one launch (start us, length us, event | category | flops | bytes accessed | tf_op | source)
XLA Modules:
  0.0 656.6 jit_solution(17741494576442215457)
XLA Ops:
  6.5 1.2 fusion.42
  7.8 1.7 fusion.44
  9.5 0.7 convert_element_type.118
  10.2 1.1 copy.62
  11.3 0.7 multiply_cosine_fusion
  12.1 26.5 %all-gather.1 = bf16[32,192,32]{1,2,0:T(8,128)(2,1)S(1)} all-gather(bf16[1,192,32]{1,2,0:T(8,128)(2,1)S(1)} %maximum_bitcast_fusion), channel_id=1, replica_groups=mesh['sp'=32,'tp'=4] {'sp'}, dimensions={0}, use_global_device_ids=true | all-gather | bytes 405504 | tf_op jit(solution)/shard_map/all_gather | solution.py:150
  38.9 1.3 reshape.267
  40.2 1.0 copy.60
  41.2 0.8 subtract_convert_fusion
  42.0 19.7 %all-gather.6.cloned.1.call-done = bf16[6144,512]{1,0:T(8,128)(2,1)} async-done(((bf16[192,512]{1,0:T(8,128)(2,1)}), bf16[6144,512]{1,0:T(8,128)(2,1)}) %all-gather.6.cloned.1.call-update) | async-done | bytes 6291472 | tf_op jit(solution)/shard_map/all_gather | solution.py:149
  61.7 1.1 broadcast_in_dim.34
  62.9 22.6 %while.18 = (s32[]{:T(128)}, f32[16,192]{1,0:T(8,128)S(1)}, f32[16,192]{1,0:T(8,128)S(1)}, f32[16,192,64]{1,2,0:T(8,128)}, s32[]{:T(128)}, /*index=5*/bf16[6144,...) while((s32[]{:T(128)}, f32[16,192]{1,0:T(8,128)S(1)}, ...), condition=%wide.region_6.7_spmd.clone, body=%wide.region_1.6_spmd.clone.sunk | while | flops 1591188224 | bytes 74948008 | solution.py:165
  62.9 22.1 %conditional.3 = ((f32[16,192]{1,0:T(8,128)S(1)}, f32[16,192]{1,0:T(8,128)S(1)}, f32[16,192,64]{1,2,0:T(8,128)})) conditional(s32[]{:T(128)} %convert_element_type.188, (f32[16,192]{1,0:T(8,128)S(1)}, f32[16,192]{1,0:T(8,128)S(1)}, f32[16,192,64]{1,2,0:T(8,128)}) %tuple.60, (s32[]{:T(128)}, s32[]{:T(128)}, bf16[6144,512]{1,0:T(8,128)(2,1)}, ...), branch_computations={%region_2.0_spmd, %region_3.5_spmd} | conditional | flops 1591188224 | bytes 74946960 | solution.py:158
  62.9 3.2 convolution_convert_fusion.1
  66.1 1.5 copy.58
  67.6 2.1 fusion.59
  69.8 2.9 fusion.58
  72.7 1.6 fusion.5
  74.3 1.0 copy-done.1
  75.4 2.8 convolution_convert_fusion
  78.1 1.5 copy.59
  79.6 5.4 fusion.9
  85.5 1.3 divide_convert_fusion
  86.8 6.4 convolution_convert_fusion.5
  93.2 4.5 all-to-all-start
  98.9 20.2 %all-to-all-done = bf16[4,48,4096]{2,1,0:T(8,128)(2,1)} async-done(((bf16[4,48,4096]{2,1,0:T(8,128)(2,1)}), bf16[4,48,4096]{2,1,0:T(8,128)(2,1)}, u32[]{:S(2)}, u32[]{:S(2)}) %all-to-all-start) | async-done | bytes 1572896 | tf_op jit(solution)/shard_map/all_to_all | solution.py:23
  119.1 1.7 convert_reduce_fusion
  121.6 1.8 convolution_convert_fusion.3
  123.4 3.5 reshape.247
  126.9 275.5 %all_to_all.15 = bf16[32,6,4096]{2,1,0:T(8,128)(2,1)S(1)} all-to-all(bf16[32,6,4096]{2,1,0:T(8,128)(2,1)} %reshape.247), channel_id=1, replica_groups=mesh['sp'=32,'tp'=4] {'sp'}, dimensions={0} | all-to-all | bytes 3145728 | tf_op jit(solution)/shard_map/all_to_all | solution.py:184
  402.3 2.1 copy.66
  405.2 60.8 %all-gather.10.cloned.1.call-done = bf16[128,6,4096]{2,0,1:T(8,128)(2,1)} async-done(((bf16[32,6,4096]{2,0,1:T(8,128)(2,1)}), bf16[128,6,4096]{2,0,1:T(8,128)(2,1)}) %all-gather.10.cloned.1.call-update) | async-done | bytes 6291472 | tf_op jit(solution)/shard_map/all_gather | solution.py:185
  466.1 9.6 %copy.67 = bf16[128,6,4096]{2,1,0:T(8,128)(2,1)} copy(bf16[128,6,4096]{2,0,1:T(8,128)(2,1)} %all-gather.10.cloned.1.call-done) | data formatting | bytes 12582912 | tf_op jit(solution)/shard_map/all_gather | solution.py:185
  475.6 10.3 %reshape.248 = bf16[768,4096]{1,0:T(8,128)(2,1)} reshape(bf16[128,6,4096]{2,1,0:T(8,128)(2,1)} %copy.67) | data formatting | bytes 12582912 | tf_op jit(solution)/shard_map/reshape | solution.py:188
  486.0 6.2 fusion.22
  492.2 12.8 %convolution_convert_fusion.2 = bf16[768,4096]{1,0:T(8,128)(2,1)} fusion(bf16[1,256,4096]{2,1,0:T(8,128)(2,1)S(1)} %copy-done, bf16[768,4096]{1,0:T(8,128)(2,1)} %reshape.248, bf16[1,4096,256]{2,1,0:T(8,128)(2,1)} %param.38, f32[768,256]{1,0:T(8,128)} %fusion.22), kind=kOutput, calls=%fused_computation.25 | convolution fusion | flops 3225550848 | bytes 17563648 | tf_op jit(solution)/shard_map/dot_general | solution.py:57
  505.0 10.1 %reshape.249 = bf16[4,32,6,4096]{3,2,1,0:T(8,128)(2,1)} reshape(bf16[768,4096]{1,0:T(8,128)(2,1)} %convolution_convert_fusion.2) | data formatting | bytes 12582912 | tf_op jit(solution)/shard_map/reshape | solution.py:193
  515.4 2.6 fusion.60
  518.1 5.7 convolution_convert_fusion.4
  523.8 72.6 %reduce-scatter.5.cloned.1.call-done = bf16[1,32,6,4096]{3,2,1,0:T(8,128)(2,1)} async-done(((bf16[4,32,6,4096]{3,2,1,0:T(8,128)(2,1)}), bf16[1,32,6,4096]{3,2,1,0:T(8,128)(2,1)}) %reduce-scatter.5.cloned.1.call-update) | async-done | bytes 1572880 | tf_op jit(solution)/shard_map/reduce_scatter | solution.py:192
  596.5 7.5 %all-to-all-start.2 = ((bf16[1,32,6,4096]{3,2,0,1:T(8,128)(2,1)}), bf16[1,32,6,4096]{3,2,0,1:T(8,128)(2,1)}, u32[]{:S(2)}, u32[]{:S(2)}) async-start(bf16[1,32,6,4096]{3,2,0,1:T(8,128)(2,1)} %bitcast.77), calls=%async_computation.4 | async-start | bytes 4194304 | tf_op jit(solution)/shard_map/all_to_all | solution.py:207
  604.2 29.8 %all-to-all-done.2 = bf16[1,32,6,4096]{3,2,0,1:T(8,128)(2,1)} async-done(((bf16[1,32,6,4096]{3,2,0,1:T(8,128)(2,1)}), bf16[1,32,6,4096]{3,2,0,1:T(8,128)(2,1)}, u32[]{:S(2)}, u32[]{:S(2)}) %all-to-all-start.2) | async-done | bytes 1572896 | tf_op jit(solution)/shard_map/all_to_all | solution.py:207
  634.0 3.7 reshape.250
  637.7 3.4 gather_fusion
  641.1 2.1 reshape.255
  643.2 3.6 multiply_reduce_fusion
  646.9 1.2 multiply_reduce_fusion.1
  648.1 1.9 fusion.36
  (89 shorter events, 3.9 us)
Async XLA Ops:
  6.5 485.7 %copy-start = (bf16[1,256,4096]{2,1,0:T(8,128)(2,1)S(1)}, bf16[1,256,4096]{2,1,0:T(8,128)(2,1)}, u32[]{:S(2)}) copy-start(bf16[1,256,4096]{2,1,0:T(8,128)(2,1)} %param.39) | copy-start | bytes 6291460
  6.5 33.6 %copy-start.3 = (bf16[192,1024]{1,0:T(8,128)(2,1)S(1)}, bf16[192,1024]{1,0:T(8,128)(2,1)}, u32[]{:S(2)}) copy-start(bf16[192,1024]{1,0:T(8,128)(2,1)} %param.24) | copy-start | bytes 1179652
  6.5 55.2 %all-gather.6.cloned.1.call-start = ((), (), s32[]{:S(2)}) async-start(), calls=%async_computation.5 | async-start | bytes 6488064 | tf_op jit(solution)/shard_map/all_gather | solution.py:149
  72.6 2.7 copy-start.1
  72.7 2.7 copy-start.10
  93.2 4.7 copy-start.8
  93.2 25.9 %all-to-all-start = ((bf16[4,48,4096]{2,1,0:T(8,128)(2,1)}), bf16[4,48,4096]{2,1,0:T(8,128)(2,1)}, u32[]{:S(2)}, u32[]{:S(2)}) async-start(bf16[4,48,4096]{2,1,0:T(8,128)(2,1)} %bitcast.75), calls=%async_computation | async-start | bytes 3145728 | tf_op jit(solution)/shard_map/all_to_all | solution.py:23
  97.7 23.4 %copy-start.4 = (bf16[48,4096]{1,0:T(8,128)(2,1)S(1)}, bf16[48,4096]{1,0:T(8,128)(2,1)}, u32[]{:S(2)}) copy-start(bf16[48,4096]{1,0:T(8,128)(2,1)} %param.32) | copy-start | bytes 1179652
  97.7 23.4 %copy-start.5 = (f32[4096]{0:T(1024)S(1)}, f32[4096]{0:T(1024)}, u32[]{:S(2)}) copy-start(f32[4096]{0:T(1024)} %param.33) | copy-start | bytes 49156
  97.7 368.4 %all-gather.10.cloned.1.call-start = ((), (), s32[]{:S(2)}) async-start(), calls=%async_computation.9 | async-start | bytes 7864320 | tf_op jit(solution)/shard_map/all_gather | solution.py:185
  98.9 22.5 %copy-start.7 = (f32[4096]{0:T(1024)S(1)}, f32[4096]{0:T(1024)}, u32[]{:S(2)}) copy-start(f32[4096]{0:T(1024)} %param.34) | copy-start | bytes 49156
  121.6 5.3 copy-start.2
  404.5 111.0 %all-gather.8.cloned.1.call-start = ((), (), s32[]{:S(2)}) async-start(), calls=%async_computation.6 | async-start | bytes 1966080 | tf_op jit(solution)/shard_map/all_gather | solution.py:186
  405.2 191.3 %reduce-scatter.5.cloned.1.call-start = ((), (), s32[]{:S(2)}) async-start(), calls=%async_computation.8 | async-start | bytes 10485760 | tf_op jit(solution)/shard_map/reduce_scatter | solution.py:192
  515.1 131.7 %reduce-scatter.3.cloned.1.call-start = ((), (), s32[]{:S(2)}) async-start(), calls=%async_computation.7 | async-start | bytes 1966080 | tf_op jit(solution)/shard_map/reduce_scatter | solution.py:198
  596.5 7.6 %copy-start.9 = (f32[48,2]{0,1:T(2,128)S(1)}, f32[48,2]{0,1:T(2,128)}, u32[]{:S(2)}) copy-start(f32[48,2]{0,1:T(2,128)} %param.36) | copy-start | bytes 1156
  596.5 37.6 %all-to-all-start.2 = ((bf16[1,32,6,4096]{3,2,0,1:T(8,128)(2,1)}), bf16[1,32,6,4096]{3,2,0,1:T(8,128)(2,1)}, u32[]{:S(2)}, u32[]{:S(2)}) async-start(bf16[1,32,6,4096]{3,2,0,1:T(8,128)(2,1)} %bitcast.77), calls=%async_computation.4 | async-start | bytes 4194304 | tf_op jit(solution)/shard_map/all_to_all | solution.py:207
  643.2 4.9 copy-start.6
Sparse Core Ops, SparseCore 0:
  9.6 52.0 all-gather.5
  404.6 61.4 all-gather.9
  467.8 27.0 all-gather.7
  515.3 81.1 reduce-scatter.4
  598.7 25.3 reduce-scatter.2
where the time goes:
time: 661 us; the launch traced here: 657 us
  blocking collectives  302 us (46%)
  waiting for transfers between devices  204 us (31%)
  local copies, waits for them, and re-layouts  54.2 us (8%)
  matrix products  51.7 us (8%)
  other arithmetic  18.1 us (3%)
  between operations  13.4 us (2%)
  starting transfers between devices  12.5 us (2%)
    all_to_all x1, blocking collectives, on_device(): lax.all_to_all(own_table, 'sp', split_axis=0, concat_axis=0, tiled=True)  275 us
    reduce_scatter x1, waiting for transfers between devices, on_device(): lax.psum_scatter(expert_out.reshape(column.shape).astype(jnp.float32).ast...  72.6 us
    all_gather x1, waiting for transfers between devices, on_device(): column = lax.all_gather(arrived[None], 'tp', axis=0, tiled=True)  60.8 us
    all_to_all x1, waiting for transfers between devices, on_device(): lax.all_to_all(routed_sum.astype(jnp.bfloat16), 'sp', split_axis=1, conca...  29.8 us
    all_gather x1, blocking collectives, on_device(): rotary_piece = lax.all_gather(key_rot, 'sp', axis=0, tiled=True)  26.5 us
    all_to_all x1, waiting for transfers between devices, sum_at_owner(): lax.all_to_all(cut_along(array, dim, count), axis, 0, 0, tiled=True)  20.2 us
    all_gather x1, waiting for transfers between devices, on_device(): latent_piece = lax.all_gather(latent_normed, 'sp', axis=0, tiled=True)  19.7 us
    dot_general x2, matrix products, expert_block(): jnp.dot(hidden, down_part, preferred_element_type=jnp.float32)  18.5 us
  transfers between devices with their start and end apart: 7, of which 5 were waited for; matrix products, arithmetic and copies ran while one was open for 12% of the time, Pallas kernels for 0%

commit v1 on v0

--- a/solution.py
+++ b/solution.py
@@ -182,7 +182,16 @@
     capacity = max(2, 2 * rows_here * TOP_K // experts)
     own_table, target = dispatch_table(normed, routes, experts, capacity)
     arrived = lax.all_to_all(own_table, "sp", split_axis=0, concat_axis=0, tiled=True)
-    column = lax.all_gather(arrived[None], "tp", axis=0, tiled=True)
+    vals = arrived[None]
+    column = jnp.concatenate(
+        lax.all_to_all(
+            jnp.stack([vals for _ in range(lax.axis_size("tp"))]),
+            axis_name="tp",
+            split_axis=0,
+            concat_axis=0,
+        ),
+        axis=0,
+    )
     group_normed = lax.all_gather(normed, "tp", axis=0, tiled=True)
     expert_out = expert_block(
         column.reshape(-1, MODEL_DIM), expert_gate[0], expert_up[0], expert_down[0]

time: 661 us -> 687 us (1.039)
  waiting for transfers between devices: 204 us -> 222 us
    all_to_all x0 -> x1, waiting for transfers between devices: none -> 83.7 us  [on_device(): lax.all_to_all(jnp.stack([vals for _ in range(lax.axis_size('tp'))]), axi...]
    all_gather x1 -> x0, waiting for transfers between devices: 60.8 us -> none  [on_device(): column = lax.all_gather(arrived[None], 'tp', axis=0, tiled=True)]
    another operation x0 -> x2, local copies, waits for them, and re-layouts: none -> 13.7 us  [the longest x1 10.2 us: on_device(): column.reshape(-1, MODEL_DIM)]
    reshape x1 -> x0, local copies, waits for them, and re-layouts: 10.3 us -> none  [on_device(): column.reshape(-1, MODEL_DIM)]
    all_to_all x0 -> x1, local copies, waits for them, and re-layouts: none -> 9.8 us  [on_device(): lax.all_to_all(jnp.stack([vals for _ in range(lax.axis_size('tp'))]), axi...]
    all_gather x1 -> x0, local copies, waits for them, and re-layouts: 9.55 us -> none  [on_device(): column = lax.all_gather(arrived[None], 'tp', axis=0, tiled=True)]
  transfers between devices with their start and end apart: 7 -> 7, of which waited for: 5 -> 5; matrix products, arithmetic and copies ran while one was open for 12% -> 11% of each run, Pallas kernels for 0% -> 0%
where the time goes in v1:
time: 687 us; the launch traced here: 683 us
  blocking collectives  302 us (44%)
  waiting for transfers between devices  222 us (32%)
  local copies, waits for them, and re-layouts  56.7 us (8%)
  matrix products  52.3 us (8%)
  other arithmetic  18.1 us (3%)
  starting transfers between devices  17.8 us (3%)
  between operations  13.4 us (2%)
    all_to_all x1, blocking collectives, on_device(): lax.all_to_all(own_table, 'sp', split_axis=0, concat_axis=0, tiled=True)  276 us
    all_to_all x1, waiting for transfers between devices, on_device(): lax.all_to_all(jnp.stack([vals for _ in range(lax.axis_size('tp'))]), axi...  83.7 us
    reduce_scatter x1, waiting for transfers between devices, on_device(): lax.psum_scatter(expert_out.reshape(column.shape).astype(jnp.float32).ast...  67.3 us
    all_to_all x1, waiting for transfers between devices, on_device(): lax.all_to_all(routed_sum.astype(jnp.bfloat16), 'sp', split_axis=1, conca...  29.8 us
    all_gather x1, blocking collectives, on_device(): rotary_piece = lax.all_gather(key_rot, 'sp', axis=0, tiled=True)  26.5 us
    all_to_all x1, waiting for transfers between devices, sum_at_owner(): lax.all_to_all(cut_along(array, dim, count), axis, 0, 0, tiled=True)  20.3 us
    all_gather x1, waiting for transfers between devices, on_device(): latent_piece = lax.all_gather(latent_normed, 'sp', axis=0, tiled=True)  19.7 us
    dot_general x2, matrix products, expert_block(): jnp.dot(hidden, down_part, preferred_element_type=jnp.float32)  19.2 us
  transfers between devices with their start and end apart: 7, of which 5 were waited for; matrix products, arithmetic and copies ran while one was open for 11% of the time, Pallas kernels for 0%

profile of v1, /device:TPU:0, one launch (start us, length us, event | category | flops | bytes accessed | tf_op | source)
XLA Modules:
  0.0 682.7 jit_solution(4934235441943498194)
XLA Ops:
  6.5 1.2 fusion.42
  7.8 1.7 fusion.44
  10.2 1.1 copy.62
  12.1 26.5 %all-gather = bf16[32,192,32]{1,2,0:T(8,128)(2,1)S(1)} all-gather(bf16[1,192,32]{1,2,0:T(8,128)(2,1)S(1)} %maximum_bitcast_fusion), channel_id=1, replica_groups=mesh['sp'=32,'tp'=4] {'sp'}, dimensions={0}, use_global_device_ids=true | all-gather | bytes 405504 | tf_op jit(solution)/shard_map/all_gather | solution.py:150
  38.9 1.3 reshape.263
  40.2 1.0 copy.60
  41.2 0.8 subtract_convert_fusion
  42.0 19.7 %all-gather.4.cloned.1.call-done = bf16[6144,512]{1,0:T(8,128)(2,1)} async-done(((bf16[192,512]{1,0:T(8,128)(2,1)}), bf16[6144,512]{1,0:T(8,128)(2,1)}) %all-gather.4.cloned.1.call-update) | async-done | bytes 6291472 | tf_op jit(solution)/shard_map/all_gather | solution.py:149
  61.7 1.1 broadcast_in_dim.32
  62.9 22.6 %while.18 = (s32[]{:T(128)}, f32[16,192]{1,0:T(8,128)S(1)}, f32[16,192]{1,0:T(8,128)S(1)}, f32[16,192,64]{1,2,0:T(8,128)}, s32[]{:T(128)}, /*index=5*/bf16[6144,...) while((s32[]{:T(128)}, f32[16,192]{1,0:T(8,128)S(1)}, ...), condition=%wide.region_6.7_spmd.clone, body=%wide.region_1.6_spmd.clone.sunk | while | flops 1591188224 | bytes 74948008 | solution.py:165
  62.9 22.1 %conditional.3 = ((f32[16,192]{1,0:T(8,128)S(1)}, f32[16,192]{1,0:T(8,128)S(1)}, f32[16,192,64]{1,2,0:T(8,128)})) conditional(s32[]{:T(128)} %convert_element_type.188, (f32[16,192]{1,0:T(8,128)S(1)}, f32[16,192]{1,0:T(8,128)S(1)}, f32[16,192,64]{1,2,0:T(8,128)}) %tuple.60, (s32[]{:T(128)}, s32[]{:T(128)}, bf16[6144,512]{1,0:T(8,128)(2,1)}, ...), branch_computations={%region_2.0_spmd, %region_3.5_spmd} | conditional | flops 1591188224 | bytes 74946960 | solution.py:158
  62.9 3.2 convolution_convert_fusion.1
  66.1 1.5 copy.58
  67.6 2.1 fusion.59
  69.8 2.9 fusion.58
  72.7 1.6 fusion.5
  74.3 1.0 copy-done.1
  75.4 2.7 convolution_convert_fusion
  78.1 1.5 copy.59
  79.6 5.4 fusion.9
  85.5 1.3 divide_convert_fusion
  86.8 6.4 convolution_convert_fusion.5
  93.2 4.6 all-to-all-start
  98.9 20.3 %all-to-all-done = bf16[4,48,4096]{2,1,0:T(8,128)(2,1)} async-done(((bf16[4,48,4096]{2,1,0:T(8,128)(2,1)}), bf16[4,48,4096]{2,1,0:T(8,128)(2,1)}, u32[]{:S(2)}, u32[]{:S(2)}) %all-to-all-start) | async-done | bytes 1572896 | tf_op jit(solution)/shard_map/all_to_all | solution.py:23
  119.1 1.7 convert_reduce_fusion
  121.6 1.8 convolution_convert_fusion.3
  123.4 3.5 reshape.246
  126.9 275.7 %all_to_all.20 = bf16[32,6,4096]{2,1,0:T(8,128)(2,1)S(1)} all-to-all(bf16[32,6,4096]{2,1,0:T(8,128)(2,1)} %reshape.246), channel_id=1, replica_groups=mesh['sp'=32,'tp'=4] {'sp'}, dimensions={0} | all-to-all | bytes 3145728 | tf_op jit(solution)/shard_map/all_to_all | solution.py:184
  402.6 0.9 copy.66
  403.4 3.5 stack.3
  406.9 5.2 all-to-all-start.2
  413.0 83.7 %all-to-all-done.2 = bf16[4,1,32,6,4096]{4,2,3,1,0:T(8,128)(2,1)} async-done(((bf16[4,1,32,6,4096]{4,2,3,1,0:T(8,128)(2,1)}), bf16[4,1,32,6,4096]{4,2,3,1,0:T(8,128)(2,1)}, u32[]{:S(2)}, u32[]{:S(2)}) %all-to-all-start.2) | async-done | bytes 6291488 | tf_op jit(solution)/shard_map/all_to_all | solution.py:187
  496.7 9.8 %copy.67 = bf16[4,1,32,6,4096]{4,3,2,0,1:T(8,128)(2,1)} copy(bf16[4,1,32,6,4096]{4,2,3,1,0:T(8,128)(2,1)} %all-to-all-done.2) | data formatting | bytes 12582912 | tf_op jit(solution)/shard_map/all_to_all | solution.py:187
  506.5 10.2 %reshape_reshape.3 = bf16[768,4096]{1,0:T(8,128)(2,1)} reshape(bf16[4,1,32,6,4096]{4,3,2,0,1:T(8,128)(2,1)} %copy.67) | data formatting | bytes 12582912 | tf_op jit(solution)/shard_map/reshape;reshape | solution.py:197
  516.7 6.2 fusion.22
  522.9 12.8 %convolution_convert_fusion.2 = bf16[768,4096]{1,0:T(8,128)(2,1)} fusion(bf16[1,256,4096]{2,1,0:T(8,128)(2,1)S(1)} %copy-done, bf16[768,4096]{1,0:T(8,128)(2,1)} %reshape_reshape.3, bf16[1,4096,256]{2,1,0:T(8,128)(2,1)} %param.38, f32[768,256]{1,0:T(8,128)} %fusion.22), kind=kOutput, calls=%fused_computation.25 | convolution fusion | flops 3225550848 | bytes 17563648 | tf_op jit(solution)/shard_map/dot_general | solution.py:57
  535.7 10.1 %reshape.247 = bf16[4,32,6,4096]{3,2,1,0:T(8,128)(2,1)} reshape(bf16[768,4096]{1,0:T(8,128)(2,1)} %convolution_convert_fusion.2) | data formatting | bytes 12582912 | tf_op jit(solution)/shard_map/reshape | solution.py:202
  546.1 2.6 fusion.60
  548.8 6.4 convolution_convert_fusion.4
  555.2 67.3 %reduce-scatter.5.cloned.1.call-done = bf16[1,32,6,4096]{3,2,1,0:T(8,128)(2,1)} async-done(((bf16[4,32,6,4096]{3,2,1,0:T(8,128)(2,1)}), bf16[1,32,6,4096]{3,2,1,0:T(8,128)(2,1)}) %reduce-scatter.5.cloned.1.call-update) | async-done | bytes 1572880 | tf_op jit(solution)/shard_map/reduce_scatter | solution.py:201
  622.5 7.5 %all-to-all-start.3 = ((bf16[1,32,6,4096]{3,2,0,1:T(8,128)(2,1)}), bf16[1,32,6,4096]{3,2,0,1:T(8,128)(2,1)}, u32[]{:S(2)}, u32[]{:S(2)}) async-start(bf16[1,32,6,4096]{3,2,0,1:T(8,128)(2,1)} %bitcast.79), calls=%async_computation.5 | async-start | bytes 4194304 | tf_op jit(solution)/shard_map/all_to_all | solution.py:216
  630.3 29.8 %all-to-all-done.3 = bf16[1,32,6,4096]{3,2,0,1:T(8,128)(2,1)} async-done(((bf16[1,32,6,4096]{3,2,0,1:T(8,128)(2,1)}), bf16[1,32,6,4096]{3,2,0,1:T(8,128)(2,1)}, u32[]{:S(2)}, u32[]{:S(2)}) %all-to-all-start.3) | async-done | bytes 1572896 | tf_op jit(solution)/shard_map/all_to_all | solution.py:216
  660.1 3.7 reshape.248
  663.8 3.4 gather_fusion
  667.2 2.1 reshape.253
  669.3 3.6 multiply_reduce_fusion
  673.0 1.2 multiply_reduce_fusion.1
  674.2 1.9 fusion.36
  (89 shorter events, 5.1 us)
Async XLA Ops:
  6.5 516.4 %copy-start = (bf16[1,256,4096]{2,1,0:T(8,128)(2,1)S(1)}, bf16[1,256,4096]{2,1,0:T(8,128)(2,1)}, u32[]{:S(2)}) copy-start(bf16[1,256,4096]{2,1,0:T(8,128)(2,1)} %param.39) | copy-start | bytes 6291460
  6.5 33.6 %copy-start.3 = (bf16[192,1024]{1,0:T(8,128)(2,1)S(1)}, bf16[192,1024]{1,0:T(8,128)(2,1)}, u32[]{:S(2)}) copy-start(bf16[192,1024]{1,0:T(8,128)(2,1)} %param.24) | copy-start | bytes 1179652
  6.5 55.2 %all-gather.4.cloned.1.call-start = ((), (), s32[]{:S(2)}) async-start(), calls=%async_computation.6 | async-start | bytes 6488064 | tf_op jit(solution)/shard_map/all_gather | solution.py:149
  72.7 2.7 copy-start.1
  72.7 2.7 copy-start.10
  93.2 4.7 copy-start.8
  93.2 25.9 %all-to-all-start = ((bf16[4,48,4096]{2,1,0:T(8,128)(2,1)}), bf16[4,48,4096]{2,1,0:T(8,128)(2,1)}, u32[]{:S(2)}, u32[]{:S(2)}) async-start(bf16[4,48,4096]{2,1,0:T(8,128)(2,1)} %bitcast.77), calls=%async_computation | async-start | bytes 3145728 | tf_op jit(solution)/shard_map/all_to_all | solution.py:23
  97.9 23.2 %copy-start.4 = (bf16[48,4096]{1,0:T(8,128)(2,1)S(1)}, bf16[48,4096]{1,0:T(8,128)(2,1)}, u32[]{:S(2)}) copy-start(bf16[48,4096]{1,0:T(8,128)(2,1)} %param.32) | copy-start | bytes 1179652
  97.9 23.2 %copy-start.5 = (f32[4096]{0:T(1024)S(1)}, f32[4096]{0:T(1024)}, u32[]{:S(2)}) copy-start(f32[4096]{0:T(1024)} %param.33) | copy-start | bytes 49156
  98.9 22.6 %copy-start.7 = (f32[4096]{0:T(1024)S(1)}, f32[4096]{0:T(1024)}, u32[]{:S(2)}) copy-start(f32[4096]{0:T(1024)} %param.34) | copy-start | bytes 49156
  121.6 5.3 copy-start.2
  406.9 89.8 %all-to-all-start.2 = ((bf16[4,1,32,6,4096]{4,2,3,1,0:T(8,128)(2,1)}), bf16[4,1,32,6,4096]{4,2,3,1,0:T(8,128)(2,1)}, u32[]{:S(2)}, u32[]{:S(2)}) async-start(bf16[4,1,32,6,4096]{4,2,3,1,0:T(8,128)(2,1)} %stack.3), calls=%async_computation.3 | async-start | bytes 12582912 | tf_op jit(solution)/shard_map/all_to_all | solution.py:187
  412.2 134.0 %all-gather.6.cloned.1.call-start = ((), (), s32[]{:S(2)}) async-start(), calls=%async_computation.7 | async-start | bytes 1966080 | tf_op jit(solution)/shard_map/all_gather | solution.py:195
  412.9 209.6 %reduce-scatter.5.cloned.1.call-start = ((), (), s32[]{:S(2)}) async-start(), calls=%async_computation.9 | async-start | bytes 10485760 | tf_op jit(solution)/shard_map/reduce_scatter | solution.py:201
  545.8 127.1 %reduce-scatter.3.cloned.1.call-start = ((), (), s32[]{:S(2)}) async-start(), calls=%async_computation.8 | async-start | bytes 1966080 | tf_op jit(solution)/shard_map/reduce_scatter | solution.py:207
  622.5 7.7 %copy-start.9 = (f32[48,2]{0,1:T(2,128)S(1)}, f32[48,2]{0,1:T(2,128)}, u32[]{:S(2)}) copy-start(f32[48,2]{0,1:T(2,128)} %param.36) | copy-start | bytes 1156
  622.5 37.6 %all-to-all-start.3 = ((bf16[1,32,6,4096]{3,2,0,1:T(8,128)(2,1)}), bf16[1,32,6,4096]{3,2,0,1:T(8,128)(2,1)}, u32[]{:S(2)}, u32[]{:S(2)}) async-start(bf16[1,32,6,4096]{3,2,0,1:T(8,128)(2,1)} %bitcast.79), calls=%async_computation.5 | async-start | bytes 4194304 | tf_op jit(solution)/shard_map/all_to_all | solution.py:216
  669.3 4.9 copy-start.6
Sparse Core Ops, SparseCore 0:
  9.6 52.0 all-gather.3
  414.6 37.0 all-gather.5
  546.0 76.5 reduce-scatter.4
  624.8 25.3 reduce-scatter.2
